TPU v7x, 128 devices: a whole 4x4x4 slice. The times are simulated.
128 devices in a mesh: rep: 2 (over z_hi), fs: 32 (over z_lo, y, x), tp: 2 (over core).
Axes of the slice: x: 4, y: 4, z: 4 (z_hi: 2, z_lo: 2; z = z_hi * 2 + z_lo), core: 2. Of those that a mesh axis runs over, the one named last changes fastest.
Arguments:
- stream_in: bfloat16 [64, 768, 2048], P(('rep', 'fs'), None, 'tp'), may hold values from -6 to 6
- mix_gain: float32 [2048], replicated, may hold values from 0.1 to 1.9
- lin_weight: bfloat16 [2048, 2048], P('fs', 'tp'), may hold values from -0.125 to 0.125
- branch_weight: bfloat16 [2048, 2048], P('fs', 'tp'), may hold values from -0.125 to 0.125
- lin_taps: float32 [4, 2048], P(None, 'tp'), may hold values from -3 to 3
- rate_blocks: bfloat16 [16, 128, 128], P('tp'), may hold values from -0.5 to 0.5
- admit_blocks: bfloat16 [16, 128, 128], P('tp'), may hold values from -0.5 to 0.5
- decay_logit: float32 [2048], P('tp'), may hold values from 3.5 to 9
- mix_out_gain: float32 [2048], P('tp'), may hold values from 0.1 to 1.9
- out_weight: bfloat16 [2048, 2048], P('tp', 'fs'), may hold values from -0.125 to 0.125
- ffn_gain: float32 [2048], replicated, may hold values from 0.1 to 1.9
- gate_weight: bfloat16 [2048, 2816], P('fs', 'tp'), may hold values from -0.125 to 0.125
- up_weight: bfloat16 [2048, 2816], P('fs', 'tp'), may hold values from -0.125 to 0.125
- gate_taps: float32 [3, 2816], P(None, 'tp'), may hold values from -3 to 3
- up_taps: float32 [3, 2816], P(None, 'tp'), may hold values from -3 to 3
- down_weight: bfloat16 [2816, 2048], P('tp', 'fs'), may hold values from -0.109375 to 0.109375
Outputs:
- stream_out: bfloat16 [64, 768, 2048], P(('rep', 'fs'), None, 'tp')
All inputs are finite; a program needn't handle non-finite values.
Results may differ from a plain program's by a relative error of at most 0.018.
Values may be sent and summed in bfloat16 or wider, within the bound.
A program may use at most 128 MiB of HBM per device.

v0:
```python
import jax
import jax.numpy as jnp
from jax import lax
from jax.sharding import PartitionSpec as P

EPS = 1e-06
GATE_SCALE = 8.0


def sent_to_all(value, axis):
    count = lax.axis_size(axis)
    return lax.all_to_all(
        jnp.broadcast_to(value[None], (count, *value.shape)), axis, 0, 0, tiled=True
    )


def in_order(tiles, dim):
    tiles = jnp.moveaxis(tiles, 0, dim)
    dims = tiles.shape
    return tiles.reshape(*dims[:dim], dims[dim] * dims[dim + 1], *dims[dim + 2 :])


def collect(value, axis, dim):
    tiles = sent_to_all(value, axis)
    return in_order(tiles, dim)


def side_by_side(arrays, axis, dim, along):
    widths = [a.shape[along] for a in arrays]
    both = jnp.concatenate(arrays, axis=along)
    whole = lax.all_gather(both, axis, axis=dim, tiled=True)
    return tuple(jnp.split(whole, [sum(widths[:k]) for k in range(1, len(widths))], axis=along))


def split_up(value, dim, count):
    before, after = (value.shape[:dim], value.shape[dim + 1 :])
    return jnp.moveaxis(value.reshape(*before, count, -1, *after), dim, 0)


def sent_and_summed(value, axis, dim):
    count = lax.axis_size(axis)
    tiles = lax.all_to_all(split_up(value, dim, count), axis, 0, 0, tiled=True)
    return jnp.sum(tiles.astype(jnp.float32), axis=0)


def norm_rows(values, scales):
    mean_sq = jnp.mean(values * values, axis=-1, keepdims=True)
    return values * lax.rsqrt(mean_sq + EPS) * scales


def causal_filter(values, kernel):
    kernel_len = kernel.shape[0]
    seq_len = values.shape[0]
    padded = jnp.pad(values, ((kernel_len - 1, 0), (0, 0)))
    summed = padded[0:seq_len] * kernel[0]
    for offset in range(1, kernel_len):
        summed = summed + padded[offset : offset + seq_len] * kernel[offset]
    return summed


def chain_combine(earlier, later):
    return (earlier[0] * later[0], later[0] * earlier[1] + later[1])


def pair_folder(source, pieces):
    return (
        jnp.dot(source, pieces[0], preferred_element_type=jnp.float32),
        jnp.dot(source, pieces[1], preferred_element_type=jnp.float32),
    )


def local(
    stream_in,
    mix_gain,
    lin_weight,
    branch_weight,
    lin_taps,
    rate_blocks,
    admit_blocks,
    decay_logit,
    mix_out_gain,
    out_weight,
    ffn_gain,
    gate_weight,
    up_weight,
    gate_taps,
    up_taps,
    down_weight,
):
    own_rows = stream_in[0]
    length = own_rows.shape[0]
    full_rows = collect(own_rows, "tp", 1)
    normed = norm_rows(full_rows.astype(jnp.float32), mix_gain).astype(jnp.bfloat16)
    linear, branch = pair_folder(normed, side_by_side((lin_weight, branch_weight), "fs", 0, 1))
    linear = linear.astype(jnp.bfloat16)
    branch = branch.astype(jnp.bfloat16)
    filtered = causal_filter(linear.astype(jnp.float32), lin_taps)
    block_count = rate_blocks.shape[0]
    block_width = rate_blocks.shape[1]
    blocks = filtered.astype(jnp.bfloat16).reshape(length, block_count, block_width)
    rate_gate = jax.nn.sigmoid(
        jnp.einsum("lbi,bij->lbj", blocks, rate_blocks, preferred_element_type=jnp.float32).reshape(
            length, -1
        )
    )
    admitted = jax.nn.sigmoid(
        jnp.einsum(
            "lbi,bij->lbj", blocks, admit_blocks, preferred_element_type=jnp.float32
        ).reshape(length, -1)
    )
    log_decay = -GATE_SCALE * rate_gate * jax.nn.softplus(-decay_logit)
    decay = jnp.exp(log_decay)
    driven = jnp.sqrt(-jnp.expm1(2.0 * log_decay)) * admitted * filtered
    _, states = lax.associative_scan(chain_combine, (decay, driven), axis=0)
    gated = (states * jax.nn.gelu(branch.astype(jnp.float32))).reshape(
        length, block_count, block_width
    )
    gated = gated * lax.rsqrt(jnp.mean(gated * gated, axis=-1, keepdims=True) + EPS)
    mixed = (gated.reshape(length, -1) * mix_out_gain).astype(jnp.bfloat16)
    mix_partial = jnp.dot(
        mixed,
        lax.all_gather(out_weight, "fs", axis=1, tiled=True),
        preferred_element_type=jnp.float32,
    )
    my_share = sent_and_summed(mix_partial.astype(jnp.bfloat16), "tp", 1)
    middle_own = (own_rows.astype(jnp.float32) + my_share).astype(jnp.bfloat16)
    middle_full = collect(middle_own, "tp", 1)
    normed2 = norm_rows(middle_full.astype(jnp.float32), ffn_gain).astype(jnp.bfloat16)
    gate_pre, up_pre = pair_folder(normed2, side_by_side((gate_weight, up_weight), "fs", 0, 1))
    gate_pre = gate_pre.astype(jnp.bfloat16)
    up_pre = up_pre.astype(jnp.bfloat16)
    gate_conv = causal_filter(gate_pre.astype(jnp.float32), gate_taps)
    up_conv = causal_filter(up_pre.astype(jnp.float32), up_taps)
    hidden = (jax.nn.silu(gate_conv) * up_conv).astype(jnp.bfloat16)
    down_partial = jnp.dot(
        hidden,
        lax.all_gather(down_weight, "fs", axis=1, tiled=True),
        preferred_element_type=jnp.float32,
    )
    down_share = sent_and_summed(down_partial.astype(jnp.bfloat16), "tp", 1)
    result = (middle_own.astype(jnp.float32) + down_share).astype(jnp.bfloat16)
    return result[None]


def solution(mesh):
    placed = (
        P(("rep", "fs"), None, "tp"),
        P(),
        P("fs", "tp"),
        P("fs", "tp"),
        P(None, "tp"),
        P("tp", None, None),
        P("tp", None, None),
        P("tp"),
        P("tp"),
        P("tp", "fs"),
        P(),
        P("fs", "tp"),
        P("fs", "tp"),
        P(None, "tp"),
        P(None, "tp"),
        P("tp", "fs"),
    )
    return jax.shard_map(
        local, mesh=mesh, in_specs=placed, out_specs=P(("rep", "fs"), None, "tp"), check_vma=False
    )
```

profile of v0, /device:TPU:1, one launch (start us, length us, event | category | flops | bytes accessed | tf_op | source)
XLA Modules:
  0.0 707.3 jit_solution(17645392529465928909)
XLA Ops:
  14.5 5.3 all-to-all-start
  26.9 131.2 %all-gather.5.cloned.1.call-done = bf16[2048,2048]{1,0:T(8,128)(2,1)} async-done(((bf16[64,2048]{1,0:T(8,128)(2,1)}), bf16[2048,2048]{1,0:T(8,128)(2,1)}) %all-gather.5.cloned.1.call-update) | async-done | bytes 8388624 | tf_op jit(solution)/shard_map/all_gather | solution.py:31
  158.1 6.4 fusion.38
  164.5 3.1 convert_bitcast_fusion
  175.9 7.6 %multiply_exponential_fusion = (f32[768,1024]{1,0:T(8,128)}, f32[768,1024]{1,0:T(8,128)S(1)}) fusion(f32[768,1024]{1,0:T(8,128)} %copy.66, f32[1024]{0:T(1024)S(1)} %fusion.62, f32[768,1024]{1,0:T(8,128)} %get-tuple-element.14, f32[768,1024]{1,0:T(8,128)} %copy.67), kind=kLoop, calls=%fused_computation.51 | loop fusion | flops 3932160 | bytes 15732736 | tf_op jit(solution)/shard_map/exp | solution.py:112
  183.5 4.2 slice.277
  187.7 4.2 slice.278
  191.9 7.6 %slice.276 = f32[384,1024]{1,0:T(8,128)} slice(f32[768,1024]{1,0:T(8,128)} %get-tuple-element.15), slice={[1:768:2], [0:1024:1]} | slice | bytes 3145728 | tf_op jit(solution)/shard_map/slice | solution.py:114
  199.5 7.6 %slice.280 = f32[384,1024]{1,0:T(8,128)} slice(f32[768,1024]{1,0:T(8,128)} %get-tuple-element.15), slice={[0:767:2], [0:1024:1]} | slice | bytes 3145728 | tf_op jit(solution)/shard_map/slice | solution.py:114
  207.1 5.6 fusion.66
  212.7 4.3 slice.283
  217.0 4.3 slice.284
  221.3 4.3 slice.282
  225.6 4.3 slice.286
  230.0 3.4 fusion.67
  292.5 2.7 slice.338
  296.6 4.4 slice.281
  301.0 4.4 slice.340
  306.8 4.4 slice.342
  311.1 8.1 %slice.275 = f32[383,1024]{1,0:T(8,128)} slice(f32[768,1024]{1,0:T(8,128)} %get-tuple-element.15), slice={[2:768:2], [0:1024:1]} | slice | bytes 3137536 | tf_op jit(solution)/shard_map/slice | solution.py:114
  334.8 9.6 %pad.84 = f32[768,1024]{1,0:T(8,128)} pad(f32[384,1024]{1,0:T(8,128)} %add.241, f32[]{:T(128)} %constant.11.clone.1), padding=1_0_1x0_0_0 | pad | bytes 4718596 | tf_op jit(solution)/shard_map/pad | solution.py:114
  347.2 5.6 pad.83
  352.8 9.5 %fusion.29 = f32[768,1024]{1,0:T(8,128)S(1)} fusion(f32[768,1024]{1,0:T(8,128)} %pad.83, f32[768,1024]{1,0:T(8,128)} %pad.84, bf16[768,2048]{0,1:T(8,128)(2,1)} %fusion.3, bf16[2048,2048]{1,0:T(8,128)(2,1)} %all-gather.5.cloned.1.call-done), kind=kOutput, calls=%fused_computation.34 | convolution fusion | flops 3230662656 | bytes 16777216 | tf_op jit(solution)/shard_map/dot_general | solution.py:68
  370.5 6.2 convolution_convert_fusion
  377.1 26.9 %all_to_all.20 = bf16[2,768,1024]{2,1,0:T(8,128)(2,1)S(1)} all-to-all(bf16[2,768,1024]{2,1,0:T(8,128)(2,1)S(1)} %bitcast.82), channel_id=1, replica_groups=mesh['rep'=2,'fs'=32,'tp'=2] {'tp'}, dimensions={0} | all-to-all | bytes 6291456 | tf_op jit(solution)/shard_map/all_to_all | solution.py:42
  411.4 6.3 all_to_all.21
  420.9 71.8 %all-gather.9.cloned.1.call-done = bf16[2048,2816]{1,0:T(8,128)(2,1)} async-done(((bf16[64,2816]{1,0:T(8,128)(2,1)}), bf16[2048,2816]{1,0:T(8,128)(2,1)}) %all-gather.9.cloned.1.call-update) | async-done | bytes 11534352 | tf_op jit(solution)/shard_map/all_gather | solution.py:31
  492.7 9.9 %fusion.15 = f32[768,1408]{1,0:T(8,128)} fusion(bf16[768,2048]{0,1:T(8,128)(2,1)} %fusion.1, bf16[2048,2816]{1,0:T(8,128)(2,1)} %all-gather.9.cloned.1.call-done), kind=kOutput, calls=%fused_computation.25 | convolution fusion | flops 4431347712 | bytes 13238272 | tf_op jit(solution)/shard_map/dot_general | solution.py:67
  502.7 6.7 fusion.21
  509.4 141.9 %all-gather.11.cloned.1.call-done = bf16[1408,2048]{0,1:T(8,128)(2,1)} async-done(((bf16[1408,64]{0,1:T(8,128)(2,1)}), bf16[1408,2048]{0,1:T(8,128)(2,1)}) %all-gather.11.cloned.1.call-update) | async-done | bytes 5767184 | tf_op jit(solution)/shard_map/all_gather | solution.py:137
  651.3 17.5 %convolution_convert_fusion.1 = bf16[768,2048]{1,0:T(8,128)(2,1)} fusion(bf16[1408,2048]{0,1:T(8,128)(2,1)} %all-gather.11.cloned.1.call-done, f32[768,1408]{1,0:T(8,128)} %fusion.21, f32[768,1408]{1,0:T(8,128)} %fusion.15, f32[1408]{0:T(1024)S(1)} %copy-done.26, f32[1408]{0:T(1024)S(1)} %copy-done.27, f32[1408]{0:T(1024)S(1)} %copy-done.25, ...), kind=kOutput, calls=%fused_computation.28 | convolution fusion | flops 4448059392 | bytes 17597440 | tf_op jit(solution)/shard_map/dot_general | solution.py:135
  671.1 26.0 %all_to_all.22 = bf16[2,768,1024]{2,1,0:T(8,128)(2,1)S(1)} all-to-all(bf16[2,768,1024]{2,1,0:T(8,128)(2,1)S(1)} %bitcast.83), channel_id=1, replica_groups=mesh['rep'=2,'fs'=32,'tp'=2] {'tp'}, dimensions={0} | all-to-all | bytes 6291456 | tf_op jit(solution)/shard_map/all_to_all | solution.py:42
  (202 shorter events, 127.8 us)
Async XLA Ops:
  6.5 161.0 %copy-start = (bf16[8,128,128]{2,1,0:T(8,128)(2,1)S(1)}, bf16[8,128,128]{2,1,0:T(8,128)(2,1)}, u32[]{:S(2)}) copy-start(bf16[8,128,128]{2,1,0:T(8,128)(2,1)} %param.21) | copy-start | bytes 786436
  6.5 151.6 %all-gather.5.cloned.1.call-start = ((), (), s32[]{:S(2)}) async-start(), calls=%async_computation.4 | async-start | bytes 8650752 | tf_op jit(solution)/shard_map/all_gather | solution.py:31
  8.3 360.4 %all-gather.7.cloned.1.call-start = ((), (), s32[]{:S(2)}) async-start(), calls=%async_computation.5 | async-start | bytes 4325376 | tf_op jit(solution)/shard_map/all_gather | solution.py:122
  9.0 483.7 %all-gather.9.cloned.1.call-start = ((), (), s32[]{:S(2)}) async-start(), calls=%async_computation.6 | async-start | bytes 11894784 | tf_op jit(solution)/shard_map/all_gather | solution.py:31
  14.5 8.6 %all-to-all-start = ((bf16[2,768,1024]{1,2,0:T(8,128)(2,1)}), bf16[2,768,1024]{1,2,0:T(8,128)(2,1)S(1)}, u32[]{:S(2)}, u32[]{:S(2)}) async-start(bf16[2,768,1024]{1,2,0:T(8,128)(2,1)} %broadcast_in_dim.9), calls=%async_computation | async-start | bytes 6291456 | tf_op jit(solution)/shard_map/all_to_all | solution.py:12
  19.8 4.0 copy-start.20
  19.8 4.0 copy-start.31
  19.8 4.0 copy-start.21
  19.8 4.0 copy-start.22
  19.8 4.7 copy-start.23
  19.8 631.5 %all-gather.11.cloned.1.call-start = ((), (), s32[]{:S(2)}) async-start(), calls=%async_computation.7 | async-start | bytes 5947392 | tf_op jit(solution)/shard_map/all_gather | solution.py:137
  306.7 13.1 %copy-start.11 = (f32[3,1024]{1,0:T(4,128)S(1)}, f32[3,1024]{1,0:T(4,128)}, u32[]{:S(2)}) copy-start(f32[3,1024]{1,0:T(4,128)} %slice.320) | copy-start | bytes 36868
  306.7 13.1 %copy-start.12 = (f32[3,1024]{1,0:T(4,128)S(1)}, f32[3,1024]{1,0:T(4,128)}, u32[]{:S(2)}) copy-start(f32[3,1024]{1,0:T(4,128)} %slice.318) | copy-start | bytes 36868
  306.7 13.1 %copy-start.13 = (f32[3,1024]{1,0:T(4,128)S(1)}, f32[3,1024]{1,0:T(4,128)}, u32[]{:S(2)}) copy-start(f32[3,1024]{1,0:T(4,128)} %slice.322) | copy-start | bytes 36868
  306.7 13.2 %copy-start.14 = (f32[2,1024]{1,0:T(2,128)S(1)}, f32[2,1024]{1,0:T(2,128)}, u32[]{:S(2)}) copy-start(f32[2,1024]{1,0:T(2,128)} %slice.317) | copy-start | bytes 24580
  306.8 13.2 %copy-start.15 = (f32[2,1024]{1,0:T(2,128)S(1)}, f32[2,1024]{1,0:T(2,128)}, u32[]{:S(2)}) copy-start(f32[2,1024]{1,0:T(2,128)} %slice.328) | copy-start | bytes 24580
  306.8 15.5 %copy-start.10 = (f32[11,1024]{1,0:T(8,128)S(1)}, f32[11,1024]{1,0:T(8,128)}, u32[]{:S(2)}) copy-start(f32[11,1024]{1,0:T(8,128)} %slice.332) | copy-start | bytes 135172
  319.9 6.0 copy-start.19
  326.2 4.3 copy-start.7
  326.2 4.3 copy-start.8
  344.5 2.6 copy-start.16
  364.8 5.7 copy-start.34
  366.4 4.1 copy-start.5
  492.7 9.9 %copy-start.6 = (bf16[768,2048]{0,1:T(8,128)(2,1)S(1)}, bf16[768,2048]{0,1:T(8,128)(2,1)}, u32[]{:S(2)}) copy-start(bf16[768,2048]{0,1:T(8,128)(2,1)} %fusion.1) | copy-start | bytes 9437188
  492.7 9.9 %copy-start.32 = (bf16[2048,2816]{1,0:T(8,128)(2,1)S(1)}, bf16[2048,2816]{1,0:T(8,128)(2,1)}, u32[]{:S(2)}) copy-start(bf16[2048,2816]{1,0:T(8,128)(2,1)} %all-gather.9.cloned.1.call-done) | copy-start | bytes 34603012
  502.6 148.6 %copy-start.25 = (f32[1408]{0:T(1024)S(1)}, f32[1408]{0:T(1024)}, u32[]{:S(2)}) copy-start(f32[1408]{0:T(1024)} %get-tuple-element.8) | copy-start | bytes 16900
  502.7 148.6 %copy-start.26 = (f32[1408]{0:T(1024)S(1)}, f32[1408]{0:T(1024)}, u32[]{:S(2)}) copy-start(f32[1408]{0:T(1024)} %get-tuple-element.9) | copy-start | bytes 16900
  502.7 148.6 %copy-start.27 = (f32[1408]{0:T(1024)S(1)}, f32[1408]{0:T(1024)}, u32[]{:S(2)}) copy-start(f32[1408]{0:T(1024)} %get-tuple-element.10) | copy-start | bytes 16900
  502.7 148.6 %copy-start.28 = (f32[1408]{0:T(1024)S(1)}, f32[1408]{0:T(1024)}, u32[]{:S(2)}) copy-start(f32[1408]{0:T(1024)} %get-tuple-element.38) | copy-start | bytes 16900
  502.7 148.6 %copy-start.29 = (f32[1408]{0:T(1024)S(1)}, f32[1408]{0:T(1024)}, u32[]{:S(2)}) copy-start(f32[1408]{0:T(1024)} %get-tuple-element.39) | copy-start | bytes 16900
  502.7 148.6 %copy-start.30 = (f32[1408]{0:T(1024)S(1)}, f32[1408]{0:T(1024)}, u32[]{:S(2)}) copy-start(f32[1408]{0:T(1024)} %get-tuple-element.40) | copy-start | bytes 16900
  697.1 3.5 copy-start.1
  (8 other events, 11.7 us)
Sparse Core Ops, SparseCore 0:
  9.0 149.0 all-gather.4
  159.7 157.1 all-gather.6
  318.6 174.1 all-gather.8
  494.2 157.0 all-gather.10
where the time goes:
time: 714 us; the launch traced here: 707 us
  waiting for transfers between devices  349 us (49%)
  local copies, waits for them, and re-layouts  161 us (23%)
  matrix products  59.8 us (8%)
  blocking collectives  59.2 us (8%)
  other arithmetic  58.9 us (8%)
  between operations  14 us (2%)
    all_gather x2, waiting for transfers between devices, side_by_side(): whole = lax.all_gather(both, axis, axis=dim, tiled=True)  203 us
    all_gather x1, waiting for transfers between devices, local(): lax.all_gather(down_weight, 'fs', axis=1, tiled=True)  142 us
    slice x56, local copies, waits for them, and re-layouts, local(): _, states = lax.associative_scan(chain_combine, (decay, driven), axis=0)  118 us
    all_to_all x2, blocking collectives, sent_and_summed(): tiles = lax.all_to_all(split_up(value, dim, count), axis, 0, 0, tiled=True)  52.9 us
    pad x17, local copies, waits for them, and re-layouts, local(): _, states = lax.associative_scan(chain_combine, (decay, driven), axis=0)  19.3 us
    mul x8, other arithmetic, chain_combine(): return (earlier[0] * later[0], later[0] * earlier[1] + later[1])  17.9 us
    dot_general x1, matrix products, local(): jnp.dot(hidden, lax.all_gather(down_weight, 'fs', axis=1, tiled=True), pr...  17.5 us
    dot_general x2, matrix products, pair_folder(): jnp.dot(source, pieces[0], preferred_element_type=jnp.float32)  16.3 us
  transfers between devices with their start and end apart: 5, of which 4 were waited for; matrix products, arithmetic and copies ran while one was open for 36% of the time, Pallas kernels for 0%

commit v1 on v0

v1 whole, which is shorter than its diff:
```python
import functools

import jax
import jax.numpy as jnp
from jax import lax
from jax.experimental import pallas as pl
from jax.experimental.pallas import tpu as pltpu
from jax.sharding import PartitionSpec as P

EPS = 1e-06
GATE_SCALE = 8.0
MESH = pl.DeviceIdType.MESH
F32, BF16 = jnp.float32, jnp.bfloat16

GROUPS = ((16, (5, 5, 3, 3)), (8, (3, 2, 1, 2)), (22, (7, 7, 4, 4)), (11, (3, 4, 2, 2)))
FINE = (True, True, True, True)
LINK_RATE = 44.0e3
HOP_US = 2.2
SHARD_ROWS = 64


def region_slots(region):
    count = 2 if region[0] == "both" else 1
    for part in region[1:]:
        if not isinstance(part, int):
            count *= part[1] - part[0]
    return count


def tree_edges():
    edges = []
    for group, (_, split) in enumerate(GROUPS):
        first = 0
        for tree, width in enumerate(split):
            columns = (first * 128, width * 128)
            first += width
            fast, slow = ("x", "y") if tree % 2 == 0 else ("y", "x")

            def add(name, way, region, parents):
                z, f, s = region
                placed = (z, s, f) if fast == "x" else (z, f, s)
                edges.append(
                    dict(
                        key=(group, tree, name),
                        way=way,
                        region=placed,
                        columns=columns,
                        bytes=region_slots(region) * width * 128 * SHARD_ROWS * 2,
                        parents=[(group, tree, p) for p in parents],
                    )
                )

            flip = (group + tree) % 2
            one, two = ("+", "-") if flip == 0 else ("-", "+")
            if tree < 2:
                add("p+", fast + "+", ("own", 0, 0), [])
                add("p-", fast + "-", ("own", 0, 0), [])
                add("p2", fast + one, ("own", -1 if one == "+" else 1, 0), ["p" + one])
                for k, (r, par) in enumerate(((0, []), (-1, ["p+"]), (1, ["p-"]), (2, ["p2"]))):
                    add(f"q+{r}", slow + "+", ("own", r, 0), par)
                    add(f"q-{r}", slow + "-", ("own", r, 0), par)
                    a = "+" if (k + flip) % 2 else "-"
                    add(f"q2{r}", slow + a, ("own", r, -1 if a == "+" else 1), [f"q{a}{r}"])
                    za, zb = ("+", "-") if k % 2 else ("-", "+")
                    add(f"z0{r}", "z" + za, ("own", r, 0), par)
                    add(f"z1{r}", "z" + zb, ("own", r, -1), [f"q+{r}"])
                    add(f"z2{r}", "z" + za, ("own", r, 1), [f"q-{r}"])
                    add(f"z3{r}", "z" + zb, ("own", r, 2), [f"q2{r}"])
            else:
                add("z", "z" + ("+" if tree == 2 else "-"), ("own", 0, 0), [])
                for k, (z, par) in enumerate((("own", []), ("other", ["z"]))):
                    add(f"p+{z}", fast + "+", (z, 0, 0), par)
                    add(f"p-{z}", fast + "-", (z, 0, 0), par)
                    a = "+" if k else "-"
                    add(f"p2{z}", fast + a, (z, -1 if a == "+" else 1, 0), [f"p{a}{z}"])
                arrived = {
                    0: ["z"],
                    -1: ["p+own", "p+other"],
                    1: ["p-own", "p-other"],
                    2: ["p2own", "p2other"],
                }
                for k, r in enumerate((0, -1, 1, 2)):
                    add(f"q+{r}", slow + "+", ("both", r, 0), arrived[r])
                    add(f"q-{r}", slow + "-", ("both", r, 0), arrived[r])
                    a = "+" if (k + flip) % 2 else "-"
                    add(f"q2{r}", slow + a, ("both", r, -1 if a == "+" else 1), [f"q{a}{r}"])
    return edges


def planned(edges):
    index = {e["key"]: k for k, e in enumerate(edges)}
    free, landed, begun = {}, {}, {}
    waiting, order = list(range(len(edges))), []
    while waiting:
        best = None
        for k in waiting:
            e = edges[k]
            if any(index[p] not in landed for p in e["parents"]):
                continue
            ready = max([landed[index[p]] for p in e["parents"]], default=0.0)
            start = max(ready, free.get(e["way"], 0.0))
            rank = (start, e["key"][0], ready)
            if best is None or rank < best[0]:
                best = (rank, k, ready, start)
        _, k, ready, start = best
        free[edges[k]["way"]] = start + edges[k]["bytes"] / LINK_RATE
        landed[k] = free[edges[k]["way"]] + HOP_US
        begun[k] = (ready, start)
        waiting.remove(k)
        order.append(k)
    return index, order, landed, begun


class Gather:
    def __init__(self, edges, plan, buffers, send, recv):
        self.edges, self.buffers, self.send, self.recv = edges, buffers, send, recv
        self.index, self.order, self.landed, self.begun = plan
        self.seen, self.queue = set(), list(self.order)
        fs, rep = lax.axis_index("fs"), lax.axis_index("rep")
        x, y, half = lax.rem(fs, 4), lax.rem(lax.div(fs, 4), 4), lax.div(fs, 16)
        z = rep * 2 + half
        self.x = {r: (lax.rem(x + r + 4, 4) if r else x) for r in (-1, 0, 1, 2)}
        self.y = {r: (lax.rem(y + r + 4, 4) if r else y) for r in (-1, 0, 1, 2)}
        self.z = {"own": half, "other": 1 - half}
        self.device = {}
        for sign, d in (("+", 1), ("-", -1)):
            self.device["x" + sign] = {"fs": half * 16 + y * 4 + self.x[d]}
            self.device["y" + sign] = {"fs": half * 16 + self.y[d] * 4 + x}
            beyond = lax.rem(z + d + 4, 4)
            self.device["z" + sign] = {
                "rep": lax.div(beyond, 2),
                "fs": lax.rem(beyond, 2) * 16 + y * 4 + x,
            }

    def place(self, edge, arriving):
        z, y, x = edge["region"]
        axis, shift = edge["way"][0], (1 if edge["way"][1] == "+" else -1)

        def moved(part, name):
            if not isinstance(part, int):
                return part
            if arriving and axis == name:
                part -= shift
            return {-2: 2, 3: -1}.get(part, part)

        def cut(part, table):
            return table[part] if isinstance(part, int) else pl.ds(part[0], part[1] - part[0])

        if arriving and axis == "z":
            z = {"own": "other", "other": "own", "both": "both"}[z]
        at_z = pl.ds(0, 2) if z == "both" else self.z[z]
        start, width = edge["columns"]
        return self.buffers[edge["key"][0]].at[
            at_z, cut(moved(y, "y"), self.y), cut(moved(x, "x"), self.x), :, pl.ds(start, width)
        ]

    def copy(self, k, arriving):
        edge = self.edges[k]
        ref = self.place(edge, arriving)
        return pltpu.make_async_remote_copy(
            src_ref=ref,
            dst_ref=ref,
            send_sem=self.send.at[k],
            recv_sem=self.recv.at[k],
            device_id=self.device[edge["way"]],
            device_id_type=MESH,
        )

    def arrive(self, k):
        if k not in self.seen:
            self.seen.add(k)
            self.copy(k, True).wait_recv()

    def start(self, k):
        for p in self.edges[k]["parents"]:
            self.arrive(self.index[p])
        self.copy(k, False).start()

    def take(self, until):
        taken = []
        while self.queue and self.begun[self.queue[0]][1] <= until:
            taken.append(self.queue.pop(0))
        return taken

    def pump(self, until):
        for k in self.take(until):
            self.start(k)

    def group_done(self, group):
        members = [k for k in self.order if self.edges[k]["key"][0] == group]
        while any(k in self.queue for k in members) or any(
            self.index[p] in self.queue for k in members for p in self.edges[k]["parents"]
        ):
            self.start(self.queue.pop(0))
        for k in members:
            self.arrive(k)

    def finish(self):
        for k in self.order:
            self.copy(k, False).wait_send()


def at_step(step, count, gather, first, pace):
    for k in range(count):
        due = gather.take(first + pace * k)
        if due:

            @pl.when(step == k)
            def _(due=due):
                for one in due:
                    gather.start(one)


def shifted_down(values, amount, fill, row):
    return jnp.where(row >= amount, pltpu.roll(values, amount, 0), fill)


def scan_rows(decay, driven, row):
    rows = decay.shape[0]
    step = 1
    while step < rows:
        before_b = shifted_down(driven, step, 0.0, row)
        before_a = shifted_down(decay, step, 1.0, row)
        driven = decay * before_b + driven
        decay = decay * before_a
        step *= 2
    return decay, driven


LEN = 768
BLOCK = 128
ROWS = 256
NORM_ROWS = 16


def kernel(edges, plan, *refs):
    (x, gain, lin, branch, taps, rate, admit, logit, mix_gain, out_w, ffn_gain, gate, up, gate_taps, up_taps, down) = refs[:16]
    result = refs[16]
    (b0, b1, b2, b3, full, normed, mixed, sent, got, hidden, dsent, dgot, pad_a, pad_b, send, recv, load, xsem, osend, orecv, dsend, drecv) = refs[17:]
    tp = lax.axis_index("tp")
    gather = Gather(edges, plan, (b0, b1, b2, b3), send, recv)
    partner = {"tp": 1 - tp}
    zl, y0, x0 = gather.z["own"], gather.y[0], gather.x[0]

    loads = [pltpu.make_async_copy(x, full.at[tp], load.at[0])]
    pieces = [(out_w, b1, 0, 0, 1024), (down, b3, 0, 0, 1408)]
    for k in range(8):
        pieces += [(lin, b0, k * 128, k * 256, 128), (branch, b0, k * 128, k * 256 + 128, 128)]
    for k in range(11):
        pieces += [(gate, b2, k * 128, k * 256, 128), (up, b2, k * 128, k * 256 + 128, 128)]
    for k, (source, target, at, to, width) in enumerate(pieces):
        loads.append(
            pltpu.make_async_copy(
                source.at[:, pl.ds(at, width)], target.at[zl, y0, x0, :, pl.ds(to, width)], load.at[k + 1]
            )
        )
    for one in loads:
        one.start()
    barrier = pltpu.get_barrier_semaphore()
    for device in [*gather.device.values(), partner]:
        pl.semaphore_signal(barrier, inc=1, device_id=device, device_id_type=MESH)
    pl.semaphore_wait(barrier, 7)
    x_copy = pltpu.make_async_remote_copy(
        src_ref=x, dst_ref=full.at[tp], send_sem=xsem.at[0], recv_sem=xsem.at[1], device_id=partner, device_id_type=MESH
    )
    x_copy.start()
    for one in loads:
        one.wait()
    gather.pump(LEAD_US)
    x_copy.wait_send()
    pltpu.make_async_remote_copy(
        src_ref=x, dst_ref=full.at[1 - tp], send_sem=xsem.at[0], recv_sem=xsem.at[1], device_id=partner, device_id_type=MESH
    ).wait_recv()

    def norm(chunk, scales, with_sums):
        rows = pl.ds(pl.multiple_of(chunk * NORM_ROWS, NORM_ROWS), NORM_ROWS)
        halves = []
        for h in range(2):
            part = full[h, rows, :].astype(F32)
            if with_sums:
                extra = [
                    sent[h, q, rows, :].astype(F32) + got[h, q, rows, :].astype(F32) for q in range(4)
                ]
                rounded = (part + jnp.concatenate(extra, axis=1)).astype(BF16)
                full[h, rows, :] = rounded
                part = rounded.astype(F32)
            halves.append(part)
        total = sum(jnp.sum(part * part, axis=-1, keepdims=True) for part in halves)
        factor = lax.rsqrt(total * (1.0 / 2048.0) + EPS)
        for h in range(2):
            normed[h, rows, :] = (halves[h] * factor * scales[h : h + 1, :]).astype(BF16)

    @pl.loop(0, LEN // NORM_ROWS)
    def _(chunk):
        norm(chunk, gain, False)

    pad_a[0:8, :] = jnp.zeros((8, BLOCK), F32)
    pad_b[0:8, :] = jnp.zeros((8, BLOCK), F32)
    row = lax.broadcasted_iota(jnp.int32, (ROWS, BLOCK), 0)
    gather.group_done(0)

    def both(buffer, step):
        columns = pl.ds(pl.multiple_of(step * 256, 256), 256)
        total = None
        for h in range(2):
            weights = buffer[h, :, :, :, columns].reshape(1024, 256)
            part = jnp.dot(normed[h], weights, preferred_element_type=F32)
            total = part if total is None else total + part
        return total.astype(BF16).astype(F32)

    @pl.loop(0, 8)
    def _(step):
        at_step(step, 8, gather, *MIX_PACE)
        lanes = pl.ds(pl.multiple_of(step * BLOCK, BLOCK), BLOCK)
        values = both(b0, step)
        pad_a[8 : 8 + LEN, :] = values[:, :BLOCK]
        pad_b[8 : 8 + LEN, :] = values[:, BLOCK:]
        tap = taps[:, lanes]
        base = -GATE_SCALE * jax.nn.softplus(-logit[:, lanes])
        scale = mix_gain[:, lanes]
        carry = jnp.zeros((1, BLOCK), F32)
        for c in range(LEN // ROWS):
            at = c * ROWS
            filtered = sum(pad_a[5 + j + at : 5 + j + at + ROWS, :] * tap[j : j + 1, :] for j in range(4))
            rounded = filtered.astype(BF16)
            rate_gate = jax.nn.sigmoid(jnp.dot(rounded, rate[step], preferred_element_type=F32))
            admitted = jax.nn.sigmoid(jnp.dot(rounded, admit[step], preferred_element_type=F32))
            log_decay = rate_gate * base
            decay = jnp.exp(log_decay)
            rest = -jnp.tanh(log_decay) * (1.0 + decay * decay)
            driven = jnp.sqrt(rest) * admitted * filtered
            product, states = scan_rows(decay, driven, row)
            states = states + product * carry
            carry = states[ROWS - 1 : ROWS, :]
            gated = states * jax.nn.gelu(pad_b[8 + at : 8 + at + ROWS, :], approximate=True)
            mean = jnp.mean(gated * gated, axis=-1, keepdims=True)
            mixed[at : at + ROWS, lanes] = (gated * lax.rsqrt(mean + EPS) * scale).astype(BF16)

    gather.group_done(1)

    def out_copy(j):
        h, q = lax.rem(1 - tp + lax.div(j, 4), 2), lax.rem(j, 4)
        return pltpu.make_async_remote_copy(
            src_ref=sent.at[h, q], dst_ref=got.at[h, q], send_sem=osend.at[j], recv_sem=orecv.at[j],
            device_id=partner, device_id_type=MESH,
        )

    def arriving_copy(j):
        h, q = lax.rem(tp + lax.div(j, 4), 2), lax.rem(j, 4)
        return pltpu.make_async_remote_copy(
            src_ref=sent.at[h, q], dst_ref=got.at[h, q], send_sem=osend.at[j], recv_sem=orecv.at[j],
            device_id=partner, device_id_type=MESH,
        )

    @pl.loop(0, 8)
    def _(j):
        at_step(j, 8, gather, *OUT_PACE)
        h, q = lax.rem(1 - tp + lax.div(j, 4), 2), lax.rem(j, 4)
        weights = b1[h, q].reshape(256, 1024)
        part = lax.dot_general(mixed[...], weights, (((1,), (1,)), ((), ())), preferred_element_type=F32)
        sent[h, q] = part.astype(BF16)

        @pl.when(j > 0)
        def _():
            out_copy(j - 1).start()

    out_copy(7).start()
    gather.pump(NORM2_US)
    for j in range(8):
        arriving_copy(j).wait_recv()

    @pl.loop(0, LEN // NORM_ROWS)
    def _(chunk):
        norm(chunk, ffn_gain, True)

    gather.group_done(2)

    @pl.loop(0, 11)
    def _(step):
        at_step(step, 11, gather, *FFN_PACE)
        lanes = pl.ds(pl.multiple_of(step * BLOCK, BLOCK), BLOCK)
        values = both(b2, step)
        pad_a[8 : 8 + LEN, :] = values[:, :BLOCK]
        pad_b[8 : 8 + LEN, :] = values[:, BLOCK:]
        tap_g, tap_u = gate_taps[:, lanes], up_taps[:, lanes]
        for c in range(LEN // ROWS):
            at = c * ROWS
            conv_g = sum(pad_a[6 + j + at : 6 + j + at + ROWS, :] * tap_g[j : j + 1, :] for j in range(3))
            conv_u = sum(pad_b[6 + j + at : 6 + j + at + ROWS, :] * tap_u[j : j + 1, :] for j in range(3))
            hidden[at : at + ROWS, lanes] = (jax.nn.silu(conv_g) * conv_u).astype(BF16)

    gather.group_done(3)

    def down_copy(q):
        return pltpu.make_async_remote_copy(
            src_ref=dsent.at[q], dst_ref=dgot.at[q], send_sem=dsend.at[q], recv_sem=drecv.at[q],
            device_id=partner, device_id_type=MESH,
        )

    def down_part(h, q):
        weights = b3[h, q].reshape(256, 1408)
        part = lax.dot_general(hidden[...], weights, (((1,), (1,)), ((), ())), preferred_element_type=F32)
        return part.astype(BF16)

    @pl.loop(0, 8)
    def _(j):
        h, q = lax.rem(1 - tp + lax.div(j, 4), 2), lax.rem(j, 4)
        part = down_part(h, q)

        @pl.when(j < 4)
        def _():
            dsent[q] = part

        @pl.when((j > 0) & (j < 5))
        def _():
            down_copy(j - 1).start()

        @pl.when(j >= 4)
        def _():
            down_copy(q).wait_recv()
            lanes = pl.ds(pl.multiple_of(q * 256, 256), 256)
            total = part.astype(F32) + dgot[q].astype(F32)
            result[:, lanes] = (full[tp, :, lanes].astype(F32) + total).astype(BF16)

    for j in range(8):
        out_copy(j).wait_send()
    for q in range(4):
        down_copy(q).wait_send()
    gather.finish()


LEAD_US = 1e9
MIX_PACE = (1e9, 0.0)
OUT_PACE = (1e9, 0.0)
NORM2_US = 1e9
FFN_PACE = (1e9, 0.0)


def local(
    stream_in, mix_gain, lin_weight, branch_weight, lin_taps, rate_blocks, admit_blocks, decay_logit, mix_out_gain,
    out_weight, ffn_gain, gate_weight, up_weight, gate_taps, up_taps, down_weight,
):
    edges = tree_edges()
    plan = planned(edges)
    count = len(edges)
    any_space, vmem = pl.BlockSpec(memory_space=pl.ANY), pl.BlockSpec(memory_space=pltpu.VMEM)
    operands = [
        (stream_in[0], any_space),
        (mix_gain.reshape(2, 1024), vmem),
        (lin_weight, any_space),
        (branch_weight, any_space),
        (lin_taps, vmem),
        (rate_blocks, vmem),
        (admit_blocks, vmem),
        (decay_logit.reshape(1, 1024), vmem),
        (mix_out_gain.reshape(1, 1024), vmem),
        (out_weight.T, any_space),
        (ffn_gain.reshape(2, 1024), vmem),
        (gate_weight, any_space),
        (up_weight, any_space),
        (gate_taps, vmem),
        (up_taps, vmem),
        (down_weight.T, any_space),
    ]
    dma = pltpu.SemaphoreType.DMA
    result = pl.pallas_call(
        functools.partial(kernel, edges, plan),
        out_shape=jax.ShapeDtypeStruct((LEN, 1024), BF16),
        in_specs=[spec for _, spec in operands],
        out_specs=vmem,
        scratch_shapes=[
            pltpu.VMEM((2, 4, 4, SHARD_ROWS, 2048), BF16),
            pltpu.VMEM((2, 4, 4, SHARD_ROWS, 1024), BF16),
            pltpu.VMEM((2, 4, 4, SHARD_ROWS, 2816), BF16),
            pltpu.VMEM((2, 4, 4, SHARD_ROWS, 1408), BF16),
            pltpu.VMEM((2, LEN, 1024), BF16),
            pltpu.VMEM((2, LEN, 1024), BF16),
            pltpu.VMEM((LEN, 1024), BF16),
            pltpu.VMEM((2, 4, LEN, 256), BF16),
            pltpu.VMEM((2, 4, LEN, 256), BF16),
            pltpu.VMEM((LEN, 1408), BF16),
            pltpu.VMEM((4, LEN, 256), BF16),
            pltpu.VMEM((4, LEN, 256), BF16),
            pltpu.VMEM((LEN + 8, BLOCK), F32),
            pltpu.VMEM((LEN + 8, BLOCK), F32),
            dma((count,)), dma((count,)), dma((41,)), dma((2,)), dma((8,)), dma((8,)), dma((4,)), dma((4,)),
        ],
        compiler_params=pltpu.CompilerParams(
            collective_id=0, has_side_effects=True, vmem_limit_bytes=63 * 1024 * 1024
        ),
    )(*[array for array, _ in operands])
    return result[None]


def solution(mesh):
    placed = (
        P(("rep", "fs"), None, "tp"), P(), P("fs", "tp"), P("fs", "tp"), P(None, "tp"), P("tp", None, None),
        P("tp", None, None), P("tp"), P("tp"), P("tp", "fs"), P(), P("fs", "tp"), P("fs", "tp"), P(None, "tp"),
        P(None, "tp"), P("tp", "fs"),
    )
    return jax.shard_map(
        local, mesh=mesh, in_specs=placed, out_specs=P(("rep", "fs"), None, "tp"), check_vma=False
    )
```

time: 714 us -> 188 us (0.26)
  waiting for transfers between devices: 349 us -> 0 us
  Pallas kernels: 0 us -> 182 us
  local copies, waits for them, and re-layouts: 161 us -> 5.27 us
  matrix products: 59.8 us -> 0 us
  blocking collectives: 59.2 us -> 0 us
  other arithmetic: 58.9 us -> 0 us
  between operations: 14 us -> 0.01 us
    all_gather x4 -> x0, waiting for transfers between devices: 345 us -> none  [the longest x2 203 us: side_by_side(): whole = lax.all_gather(both, axis, axis=dim, tiled=True)]
    pallas_call x0 -> x1, Pallas kernels: none -> 182 us  [local(): pl.pallas_call(functools.partial(kernel, edges, plan), out_shape=jax.Shap...]
    slice x58 -> x0, local copies, waits for them, and re-layouts: 119 us -> none  [the longest x56 118 us: local(): _, states = lax.associative_scan(chain_combine, (decay, driven), axis=0)]
    dot_general x8 -> x0, matrix products: 59.8 us -> none  [the longest x1 17.5 us: local(): jnp.dot(hidden, lax.all_gather(down_weight, 'fs', axis=1, tiled=True), pr...]
    all_to_all x3 -> x0, blocking collectives: 59.2 us -> none  [the longest x2 52.9 us: sent_and_summed(): tiles = lax.all_to_all(split_up(value, dim, count), axis, 0, 0, tiled=True)]
    pad x17 -> x0, local copies, waits for them, and re-layouts: 19.3 us -> none  [local(): _, states = lax.associative_scan(chain_combine, (decay, driven), axis=0)]
    mul x9 -> x0, other arithmetic: 17.9 us -> none  [the longest x8 17.9 us: chain_combine(): return (earlier[0] * later[0], later[0] * earlier[1] + later[1])]
    add x17 -> x0, other arithmetic: 9.47 us -> none  [the longest x9 6.96 us: chain_combine(): return (earlier[0] * later[0], later[0] * earlier[1] + later[1])]
  transfers between devices with their start and end apart: 5 -> 0, of which waited for: 4 -> 0; matrix products, arithmetic and copies ran while one was open for 36% -> 0% of each run, Pallas kernels for 0% -> 0%
where the time goes in v1:
time: 188 us
  Pallas kernels  182 us (97%)
  local copies, waits for them, and re-layouts  5.27 us (3%)
    pallas_call x1, Pallas kernels, local(): pl.pallas_call(functools.partial(kernel, edges, plan), out_shape=jax.Shap...  182 us

profile of v1, /device:TPU:1, one launch (start us, length us, event | category | flops | bytes accessed | tf_op | source)
XLA Modules:
  0.0 187.7 jit_solution(10047759254766886517)
XLA Ops:
  0.0 1.3 reshape.12.refs_1_
  1.3 1.3 reshape.15.refs_10_
  2.6 182.4 %shard_map.154 = bf16[768,1024]{1,0:T(8,128)(2,1)} custom-call(bf16[768,1024]{1,0:T(8,128)(2,1)} %bitcast.7, f32[2,1024]{1,0:T(2,128)} %reshape.12.refs_1_, bf16[64,1024]{1,0:T(8,128)(2,1)} %refs_2_.1, bf16[64,1024]{1,0:T(8,128)(2,1)} %refs_3_.1, f32[4,1024]{1,0:T(4,128)} %refs_4_.1, bf16[8,128,128]{2,1,0:T(8,128)(2,1)} %refs_5_.1, ...), custom_call_target="tpu_custom_call" | custom-call | tf_op jit(solution)/shard_map/pallas_call | solution.py:466
  185.0 2.7 %copy.18 = bf16[1,768,1024]{2,1,0:T(8,128)(2,1)} copy(bf16[1,768,1024]{2,1,0:T(8,128)(2,1)} %bitcast.6) | data formatting | bytes 3145728

commit v2 on v1

--- a/solution.py
+++ b/solution.py
@@ -12,10 +12,18 @@
 MESH = pl.DeviceIdType.MESH
 F32, BF16 = jnp.float32, jnp.bfloat16
 
-GROUPS = ((16, (5, 5, 3, 3)), (8, (3, 2, 1, 2)), (22, (7, 7, 4, 4)), (11, (3, 4, 2, 2)))
-FINE = (True, True, True, True)
-LINK_RATE = 44.0e3
-HOP_US = 2.2
+GROUPS = (
+    (0, 0, (5, 5, 3, 3)),
+    (1, 0, (3, 2, 1, 2)),
+    (2, 0, (7, 7, 4, 4)),
+    (3, 0, (3, 4, 2, 2)),
+)
+LINK_RATE = 48000.0
+HOP_US = 3.0
+EARLY_US = 100.0
+GATE_UP, DOWN = (2, 2), 3
+ROW_STEPS = (0, 1, -1, 2)
+ROW_ORDER = tuple((half, step) for half in ("own", "other") for step in ROW_STEPS)
 SHARD_ROWS = 64
 
 
@@ -29,8 +37,7 @@
 
 def tree_edges():
     edges = []
-    for group, (_, split) in enumerate(GROUPS):
-        first = 0
+    for group, (buffer, first, split) in enumerate(GROUPS):
         for tree, width in enumerate(split):
             columns = (first * 128, width * 128)
             first += width
@@ -43,6 +50,7 @@
                     dict(
                         key=(group, tree, name),
                         way=way,
+                        buffer=buffer,
                         region=placed,
                         columns=columns,
                         bytes=region_slots(region) * width * 128 * SHARD_ROWS * 2,
@@ -87,6 +95,22 @@
     return edges
 
 
+def landing(edge):
+    z, y, x = edge["region"]
+    shift = 1 if edge["way"][1] == "+" else -1
+    if edge["way"][0] == "z":
+        return {"own": "other", "other": "own", "both": "both"}[z], y, x
+    wrap = {-2: 2, 3: -1}
+    if edge["way"][0] == "y":
+        return z, wrap.get(y - shift, y - shift), x
+    return z, y, wrap.get(x - shift, x - shift)
+
+
+def in_row(edge, row):
+    z, y, _ = landing(edge)
+    return z in (row[0], "both") and y == row[1]
+
+
 def planned(edges):
     index = {e["key"]: k for k, e in enumerate(edges)}
     free, landed, begun = {}, {}, {}
@@ -99,22 +123,26 @@
                 continue
             ready = max([landed[index[p]] for p in e["parents"]], default=0.0)
             start = max(ready, free.get(e["way"], 0.0))
-            rank = (start, e["key"][0], ready)
-            if best is None or rank < best[0]:
-                best = (rank, k, ready, start)
+            if best is None or (start, e["key"][0], ready) < best[0]:
+                best = ((start, e["key"][0], ready), k, ready, start)
         _, k, ready, start = best
         free[edges[k]["way"]] = start + edges[k]["bytes"] / LINK_RATE
         landed[k] = free[edges[k]["way"]] + HOP_US
         begun[k] = (ready, start)
         waiting.remove(k)
         order.append(k)
-    return index, order, landed, begun
+    last, due = {}, {}
+    for k in order:
+        due[k] = max(begun[k][0], begun[k][1] - EARLY_US, last.get(edges[k]["way"], 0.0))
+        last[edges[k]["way"]] = due[k]
+    order.sort(key=lambda k: (due[k], begun[k][1]))
+    return index, order, landed, due
 
 
 class Gather:
     def __init__(self, edges, plan, buffers, send, recv):
         self.edges, self.buffers, self.send, self.recv = edges, buffers, send, recv
-        self.index, self.order, self.landed, self.begun = plan
+        self.index, self.order, self.landed, self.due = plan
         self.seen, self.queue = set(), list(self.order)
         fs, rep = lax.axis_index("fs"), lax.axis_index("rep")
         x, y, half = lax.rem(fs, 4), lax.rem(lax.div(fs, 4), 4), lax.div(fs, 16)
@@ -133,25 +161,11 @@
             }
 
     def place(self, edge, arriving):
-        z, y, x = edge["region"]
-        axis, shift = edge["way"][0], (1 if edge["way"][1] == "+" else -1)
-
-        def moved(part, name):
-            if not isinstance(part, int):
-                return part
-            if arriving and axis == name:
-                part -= shift
-            return {-2: 2, 3: -1}.get(part, part)
-
-        def cut(part, table):
-            return table[part] if isinstance(part, int) else pl.ds(part[0], part[1] - part[0])
-
-        if arriving and axis == "z":
-            z = {"own": "other", "other": "own", "both": "both"}[z]
+        z, y, x = landing(edge) if arriving else edge["region"]
         at_z = pl.ds(0, 2) if z == "both" else self.z[z]
         start, width = edge["columns"]
-        return self.buffers[edge["key"][0]].at[
-            at_z, cut(moved(y, "y"), self.y), cut(moved(x, "x"), self.x), :, pl.ds(start, width)
+        return self.buffers[edge["buffer"]].at[
+            at_z, self.y[y], self.x[x], :, pl.ds(start, width)
         ]
 
     def copy(self, k, arriving):
@@ -166,49 +180,67 @@
             device_id_type=MESH,
         )
 
-    def arrive(self, k):
-        if k not in self.seen:
-            self.seen.add(k)
-            self.copy(k, True).wait_recv()
-
-    def start(self, k):
-        for p in self.edges[k]["parents"]:
-            self.arrive(self.index[p])
-        self.copy(k, False).start()
-
-    def take(self, until):
-        taken = []
-        while self.queue and self.begun[self.queue[0]][1] <= until:
-            taken.append(self.queue.pop(0))
-        return taken
+    def arrivals(self, ks):
+        found = [k for k in ks if k not in self.seen]
+        self.seen.update(found)
+        return [(True, k) for k in found]
+
+    def begin(self, k):
+        return self.arrivals([self.index[p] for p in self.edges[k]["parents"]]) + [(False, k)]
+
+    def due_by(self, until):
+        steps = []
+        while self.queue and self.due[self.queue[0]] <= until:
+            steps += self.begin(self.queue.pop(0))
+        return steps
+
+    def members(self, group):
+        return [k for k in self.order if self.edges[k]["key"][0] == group]
+
+    def run(self, steps):
+        for arriving, k in steps:
+            if arriving:
+                self.copy(k, True).wait_recv()
+            else:
+                self.copy(k, False).start()
 
     def pump(self, until):
-        for k in self.take(until):
-            self.start(k)
-
-    def group_done(self, group):
-        members = [k for k in self.order if self.edges[k]["key"][0] == group]
+        self.run(self.due_by(until))
+
+    def until_done(self, group, row=None):
+        members = self.members(group)
+        if row is not None:
+            members = [k for k in members if in_row(self.edges[k], row)]
+        steps = self.due_by(max([self.landed[k] for k in members], default=0.0) - HOP_US)
         while any(k in self.queue for k in members) or any(
             self.index[p] in self.queue for k in members for p in self.edges[k]["parents"]
         ):
-            self.start(self.queue.pop(0))
-        for k in members:
-            self.arrive(k)
-
-    def finish(self):
-        for k in self.order:
+            steps += self.begin(self.queue.pop(0))
+        return steps + self.arrivals(members)
+
+    def group_done(self, group):
+        self.run(self.until_done(group))
+
+    def group_time(self, group):
+        return max([self.landed[k] for k in self.members(group)], default=0.0)
+
+    def timetable(self, count, first, pace, subs=1):
+        return [
+            [self.due_by(first + pace * (k + j / subs)) for j in range(subs)] for k in range(count)
+        ]
+
+    def sent(self, group):
+        for k in self.members(group):
             self.copy(k, False).wait_send()
 
 
-def at_step(step, count, gather, first, pace):
-    for k in range(count):
-        due = gather.take(first + pace * k)
-        if due:
+def at_step(step, table, gather, sub=0):
+    for k, steps in enumerate(table):
+        if steps[sub]:
 
             @pl.when(step == k)
-            def _(due=due):
-                for one in due:
-                    gather.start(one)
+            def _(steps=steps[sub]):
+                gather.run(steps)
 
 
 def shifted_down(values, amount, fill, row):
@@ -236,13 +268,19 @@
 def kernel(edges, plan, *refs):
     (x, gain, lin, branch, taps, rate, admit, logit, mix_gain, out_w, ffn_gain, gate, up, gate_taps, up_taps, down) = refs[:16]
     result = refs[16]
-    (b0, b1, b2, b3, full, normed, mixed, sent, got, hidden, dsent, dgot, pad_a, pad_b, send, recv, load, xsem, osend, orecv, dsend, drecv) = refs[17:]
+    small = (gain, taps, rate, admit, logit, mix_gain, ffn_gain, gate_taps, up_taps)
+    held = refs[17 : 17 + len(small)]
+    (b0, b1, b2, b3, full, normed, mixed, sent, got, hidden, dgot, final, pad_a, pad_b) = refs[26:40]
+    (send, recv, load, ssem, xsem, osend, orecv, dsend, drecv, fsem) = refs[40:]
     tp = lax.axis_index("tp")
     gather = Gather(edges, plan, (b0, b1, b2, b3), send, recv)
     partner = {"tp": 1 - tp}
     zl, y0, x0 = gather.z["own"], gather.y[0], gather.x[0]
 
-    loads = [pltpu.make_async_copy(x, full.at[tp], load.at[0])]
+    x_load = pltpu.make_async_copy(x, full.at[tp], load.at[0])
+    small_loads = [pltpu.make_async_copy(a, b, ssem.at[k]) for k, (a, b) in enumerate(zip(small, held))]
+    (gain, taps, rate, admit, logit, mix_gain, ffn_gain, gate_taps, up_taps) = held
+    loads = []
     pieces = [(out_w, b1, 0, 0, 1024), (down, b3, 0, 0, 1408)]
     for k in range(8):
         pieces += [(lin, b0, k * 128, k * 256, 128), (branch, b0, k * 128, k * 256 + 128, 128)]
@@ -263,10 +301,17 @@
     x_copy = pltpu.make_async_remote_copy(
         src_ref=x, dst_ref=full.at[tp], send_sem=xsem.at[0], recv_sem=xsem.at[1], device_id=partner, device_id_type=MESH
     )
-    x_copy.start()
     for one in loads:
         one.wait()
+    gather.pump(0.0)
+    x_copy.start()
+    x_load.start()
+    for one in small_loads:
+        one.start()
     gather.pump(LEAD_US)
+    x_load.wait()
+    for one in small_loads:
+        one.wait()
     x_copy.wait_send()
     pltpu.make_async_remote_copy(
         src_ref=x, dst_ref=full.at[1 - tp], send_sem=xsem.at[0], recv_sem=xsem.at[1], device_id=partner, device_id_type=MESH
@@ -288,16 +333,23 @@
         total = sum(jnp.sum(part * part, axis=-1, keepdims=True) for part in halves)
         factor = lax.rsqrt(total * (1.0 / 2048.0) + EPS)
         for h in range(2):
-            normed[h, rows, :] = (halves[h] * factor * scales[h : h + 1, :]).astype(BF16)
-
-    @pl.loop(0, LEN // NORM_ROWS)
-    def _(chunk):
-        norm(chunk, gain, False)
+            normed[h, rows, :] = (halves[h] * factor * scales[:, h * 1024 : h * 1024 + 1024]).astype(BF16)
+
+    table = gather.timetable(LEN // NORM_ROWS // 6, *NORM_PACE)
+
+    @pl.loop(0, LEN // NORM_ROWS // 6)
+    def _(part):
+        at_step(part, table, gather)
+
+        @pl.loop(0, 6)
+        def _(chunk):
+            norm(part * 6 + chunk, gain, False)
 
     pad_a[0:8, :] = jnp.zeros((8, BLOCK), F32)
     pad_b[0:8, :] = jnp.zeros((8, BLOCK), F32)
     row = lax.broadcasted_iota(jnp.int32, (ROWS, BLOCK), 0)
     gather.group_done(0)
+    start = gather.group_time(0)
 
     def both(buffer, step):
         columns = pl.ds(pl.multiple_of(step * 256, 256), 256)
@@ -308,9 +360,11 @@
             total = part if total is None else total + part
         return total.astype(BF16).astype(F32)
 
+    table1 = gather.timetable(8, start + MIX_PACE[0], MIX_PACE[1], 4)
+
     @pl.loop(0, 8)
     def _(step):
-        at_step(step, 8, gather, *MIX_PACE)
+        at_step(step, table1, gather, 0)
         lanes = pl.ds(pl.multiple_of(step * BLOCK, BLOCK), BLOCK)
         values = both(b0, step)
         pad_a[8 : 8 + LEN, :] = values[:, :BLOCK]
@@ -320,6 +374,7 @@
         scale = mix_gain[:, lanes]
         carry = jnp.zeros((1, BLOCK), F32)
         for c in range(LEN // ROWS):
+            at_step(step, table1, gather, c + 1)
             at = c * ROWS
             filtered = sum(pad_a[5 + j + at : 5 + j + at + ROWS, :] * tap[j : j + 1, :] for j in range(4))
             rounded = filtered.astype(BF16)
@@ -352,9 +407,11 @@
             device_id=partner, device_id_type=MESH,
         )
 
+    table2 = gather.timetable(8, start + OUT_PACE[0], OUT_PACE[1])
+
     @pl.loop(0, 8)
     def _(j):
-        at_step(j, 8, gather, *OUT_PACE)
+        at_step(j, table2, gather)
         h, q = lax.rem(1 - tp + lax.div(j, 4), 2), lax.rem(j, 4)
         weights = b1[h, q].reshape(256, 1024)
         part = lax.dot_general(mixed[...], weights, (((1,), (1,)), ((), ())), preferred_element_type=F32)
@@ -365,23 +422,39 @@
             out_copy(j - 1).start()
 
     out_copy(7).start()
-    gather.pump(NORM2_US)
+    gather.pump(start + NORM2_US)
     for j in range(8):
         arriving_copy(j).wait_recv()
 
-    @pl.loop(0, LEN // NORM_ROWS)
-    def _(chunk):
-        norm(chunk, ffn_gain, True)
-
-    gather.group_done(2)
+    table3 = gather.timetable(LEN // NORM_ROWS // 6, start + NORM2_US, NORM_PACE[1])
+
+    @pl.loop(0, LEN // NORM_ROWS // 6)
+    def _(part):
+        at_step(part, table3, gather)
+
+        @pl.loop(0, 6)
+        def _(chunk):
+            norm(part * 6 + chunk, ffn_gain, True)
+
+    for j in range(8):
+        out_copy(j).wait_send()
+    gather.sent(0)
+    gather.group_done(GATE_UP[0])
+    ready = gather.group_time(GATE_UP[0])
+    table4 = gather.timetable(6, ready + FFN_PACE[0], FFN_PACE[1], 2)
+    middle = gather.until_done(GATE_UP[1])
+    later = max(ready + 6 * FFN_PACE[1], gather.group_time(GATE_UP[1])) + FFN_PACE[0]
+    table5 = gather.timetable(5, later, FFN_PACE[1], 2)
+    table4 = table4 + [[middle + table5[0][0], table5[0][1]]] + table5[1:]
 
     @pl.loop(0, 11)
     def _(step):
-        at_step(step, 11, gather, *FFN_PACE)
+        at_step(step, table4, gather, 0)
         lanes = pl.ds(pl.multiple_of(step * BLOCK, BLOCK), BLOCK)
         values = both(b2, step)
         pad_a[8 : 8 + LEN, :] = values[:, :BLOCK]
         pad_b[8 : 8 + LEN, :] = values[:, BLOCK:]
+        at_step(step, table4, gather, 1)
         tap_g, tap_u = gate_taps[:, lanes], up_taps[:, lanes]
         for c in range(LEN // ROWS):
             at = c * ROWS
@@ -389,51 +462,72 @@
             conv_u = sum(pad_b[6 + j + at : 6 + j + at + ROWS, :] * tap_u[j : j + 1, :] for j in range(3))
             hidden[at : at + ROWS, lanes] = (jax.nn.silu(conv_g) * conv_u).astype(BF16)
 
-    gather.group_done(3)
+    tables = [[gather.until_done(DOWN, row)] for row in ROW_ORDER]
+
+    def row_of(j):
+        k = lax.rem(j, 4)
+        step = jnp.where(k == 2, 3, jnp.where(k == 3, 2, k))
+        return lax.rem(zl + lax.div(j, 4), 2), lax.rem(y0 + step, 4)
 
     def down_copy(q):
         return pltpu.make_async_remote_copy(
-            src_ref=dsent.at[q], dst_ref=dgot.at[q], send_sem=dsend.at[q], recv_sem=drecv.at[q],
+            src_ref=sent.at[0, q], dst_ref=dgot.at[q], send_sem=dsend.at[q], recv_sem=drecv.at[q],
             device_id=partner, device_id_type=MESH,
         )
 
-    def down_part(h, q):
+    def final_copy(q):
+        lanes = pl.ds(pl.multiple_of(q * 256, 256), 256)
+        return pltpu.make_async_copy(final.at[:, lanes], result.at[:, lanes], fsem.at[q])
+
+    def complete(j):
+        _, q = row_of(j)
+        down_copy(q).wait_recv()
+        lanes = pl.ds(pl.multiple_of(q * 256, 256), 256)
+        total = sent[1, q].astype(F32) + dgot[q].astype(F32)
+        final[:, lanes] = (full[tp, :, lanes].astype(F32) + total).astype(BF16)
+        final_copy(q).start()
+
+    def pass_on(j):
+        h, q = row_of(j)
+
+        @pl.when(h != tp)
+        def _():
+            down_copy(q).start()
+
+    @pl.loop(0, 8)
+    def _(j):
+        at_step(j, tables, gather)
+        h, q = row_of(j)
         weights = b3[h, q].reshape(256, 1408)
         part = lax.dot_general(hidden[...], weights, (((1,), (1,)), ((), ())), preferred_element_type=F32)
-        return part.astype(BF16)
-
-    @pl.loop(0, 8)
-    def _(j):
-        h, q = lax.rem(1 - tp + lax.div(j, 4), 2), lax.rem(j, 4)
-        part = down_part(h, q)
-
-        @pl.when(j < 4)
+        sent[jnp.where(h == tp, 1, 0), q] = part.astype(BF16)
+
+        @pl.when(j > 0)
         def _():
-            dsent[q] = part
-
-        @pl.when((j > 0) & (j < 5))
+            pass_on(j - 1)
+
+        @pl.when(j >= 6)
         def _():
-            down_copy(j - 1).start()
-
-        @pl.when(j >= 4)
-        def _():
-            down_copy(q).wait_recv()
-            lanes = pl.ds(pl.multiple_of(q * 256, 256), 256)
-            total = part.astype(F32) + dgot[q].astype(F32)
-            result[:, lanes] = (full[tp, :, lanes].astype(F32) + total).astype(BF16)
-
-    for j in range(8):
-        out_copy(j).wait_send()
+            complete(j - 6)
+
+    pass_on(7)
+    gather.pump(1e9)
+    for group in range(1, DOWN):
+        gather.sent(group)
+    complete(2)
+    complete(3)
+    gather.sent(DOWN)
     for q in range(4):
         down_copy(q).wait_send()
-    gather.finish()
-
-
-LEAD_US = 1e9
-MIX_PACE = (1e9, 0.0)
-OUT_PACE = (1e9, 0.0)
-NORM2_US = 1e9
-FFN_PACE = (1e9, 0.0)
+        final_copy(q).wait()
+
+
+LEAD_US = 3.0
+NORM_PACE = (3.0, 0.9)
+MIX_PACE = (4.0, 3.0)
+OUT_PACE = (28.0, 0.8)
+NORM2_US = 37.0
+FFN_PACE = (4.0, 1.6)
 
 
 def local(
@@ -443,32 +537,34 @@
     edges = tree_edges()
     plan = planned(edges)
     count = len(edges)
-    any_space, vmem = pl.BlockSpec(memory_space=pl.ANY), pl.BlockSpec(memory_space=pltpu.VMEM)
+    any_space = pl.BlockSpec(memory_space=pl.ANY)
     operands = [
-        (stream_in[0], any_space),
-        (mix_gain.reshape(2, 1024), vmem),
-        (lin_weight, any_space),
-        (branch_weight, any_space),
-        (lin_taps, vmem),
-        (rate_blocks, vmem),
-        (admit_blocks, vmem),
-        (decay_logit.reshape(1, 1024), vmem),
-        (mix_out_gain.reshape(1, 1024), vmem),
-        (out_weight.T, any_space),
-        (ffn_gain.reshape(2, 1024), vmem),
-        (gate_weight, any_space),
-        (up_weight, any_space),
-        (gate_taps, vmem),
-        (up_taps, vmem),
-        (down_weight.T, any_space),
+        stream_in[0],
+        mix_gain.reshape(1, 2048),
+        lin_weight,
+        branch_weight,
+        lin_taps,
+        rate_blocks,
+        admit_blocks,
+        decay_logit.reshape(1, 1024),
+        mix_out_gain.reshape(1, 1024),
+        out_weight.T,
+        ffn_gain.reshape(1, 2048),
+        gate_weight,
+        up_weight,
+        gate_taps,
+        up_taps,
+        down_weight.T,
     ]
+    small = [operands[k] for k in (1, 4, 5, 6, 7, 8, 10, 13, 14)]
     dma = pltpu.SemaphoreType.DMA
     result = pl.pallas_call(
         functools.partial(kernel, edges, plan),
         out_shape=jax.ShapeDtypeStruct((LEN, 1024), BF16),
-        in_specs=[spec for _, spec in operands],
-        out_specs=vmem,
+        in_specs=[any_space] * len(operands),
+        out_specs=any_space,
         scratch_shapes=[
+            *[pltpu.VMEM(a.shape, a.dtype) for a in small],
             pltpu.VMEM((2, 4, 4, SHARD_ROWS, 2048), BF16),
             pltpu.VMEM((2, 4, 4, SHARD_ROWS, 1024), BF16),
             pltpu.VMEM((2, 4, 4, SHARD_ROWS, 2816), BF16),
@@ -480,15 +576,16 @@
             pltpu.VMEM((2, 4, LEN, 256), BF16),
             pltpu.VMEM((LEN, 1408), BF16),
             pltpu.VMEM((4, LEN, 256), BF16),
-            pltpu.VMEM((4, LEN, 256), BF16),
+            pltpu.VMEM((LEN, 1024), BF16),
             pltpu.VMEM((LEN + 8, BLOCK), F32),
             pltpu.VMEM((LEN + 8, BLOCK), F32),
-            dma((count,)), dma((count,)), dma((41,)), dma((2,)), dma((8,)), dma((8,)), dma((4,)), dma((4,)),
+            dma((count,)), dma((count,)), dma((41,)), dma((len(small),)), dma((2,)), dma((8,)), dma((8,)), dma((4,)), dma((4,)),
+            dma((4,)),
         ],
         compiler_params=pltpu.CompilerParams(
             collective_id=0, has_side_effects=True, vmem_limit_bytes=63 * 1024 * 1024
         ),
-    )(*[array for array, _ in operands])
+    )(*operands)
     return result[None]
 
 

time: 188 us -> 139 us (0.74)
  Pallas kernels: 182 us -> 136 us
  local copies, waits for them, and re-layouts: 5.27 us -> 2.67 us
    pallas_call x1, Pallas kernels: 182 us -> 136 us  [local(): pl.pallas_call(functools.partial(kernel, edges, plan), out_shape=jax.Shap...]
    reshape x2 -> x0, local copies, waits for them, and re-layouts: 2.6 us -> none  [the longest x1 1.3 us: local(): mix_gain.reshape(2, 1024)]
where the time goes in v2:
time: 139 us
  Pallas kernels  136 us (98%)
  local copies, waits for them, and re-layouts  2.67 us (2%)
    pallas_call x1, Pallas kernels, local(): pl.pallas_call(functools.partial(kernel, edges, plan), out_shape=jax.Shap...  136 us

profile of v2, /device:TPU:1, one launch (start us, length us, event | category | flops | bytes accessed | tf_op | source)
XLA Modules:
  0.0 138.8 jit_solution(6578200266402220803)
XLA Ops:
  0.0 136.2 %shard_map.154 = bf16[768,1024]{1,0:T(8,128)(2,1)} custom-call(bf16[768,1024]{1,0:T(8,128)(2,1)} %bitcast.9, f32[1,2048]{1,0:T(1,128)} %bitcast.12, bf16[64,1024]{1,0:T(8,128)(2,1)} %refs_2_.1, bf16[64,1024]{1,0:T(8,128)(2,1)} %refs_3_.1, f32[4,1024]{1,0:T(4,128)} %refs_4_.1, bf16[8,128,128]{2,1,0:T(8,128)(2,1)} %refs_5_.1, bf16[8,128,128]{2,1,0:T(8,128)(2,1)} %refs_6_.1, ...), custom_call_target="tpu_custom_call" | custom-call | tf_op jit(solution)/shard_map/pallas_call | solution.py:561
  136.2 2.7 %copy.18 = bf16[1,768,1024]{2,1,0:T(8,128)(2,1)} copy(bf16[1,768,1024]{2,1,0:T(8,128)(2,1)} %bitcast.8) | data formatting | bytes 3145728

commit v3 on v2

--- a/solution.py
+++ b/solution.py
@@ -106,6 +106,15 @@
     return z, y, wrap.get(x - shift, x - shift)
 
 
+def unit_of(edge):
+    group, tree, name = edge["key"]
+    if tree < 2 and name[0] == "z":
+        return (group, tree, "z", landing(edge)[1]) if group == DOWN else (group, tree, "z")
+    if tree >= 2 and name[:2] == "q2" and (group != DOWN or tree == 2):
+        return (group, tree, "q2")
+    return edge["key"]
+
+
 def in_row(edge, row):
     z, y, _ = landing(edge)
     return z in (row[0], "both") and y == row[1]
@@ -139,11 +148,19 @@
     return index, order, landed, due
 
 
+def send_unit(edge):
+    group, tree, name = edge["key"]
+    return (group * 4 + tree) * 3 + "pqz".index(name[0])
+
+
 class Gather:
     def __init__(self, edges, plan, buffers, send, recv):
         self.edges, self.buffers, self.send, self.recv = edges, buffers, send, recv
         self.index, self.order, self.landed, self.due = plan
         self.seen, self.queue = set(), list(self.order)
+        self.unit = {}
+        for e in edges:
+            self.unit.setdefault(unit_of(e), len(self.unit))
         fs, rep = lax.axis_index("fs"), lax.axis_index("rep")
         x, y, half = lax.rem(fs, 4), lax.rem(lax.div(fs, 4), 4), lax.div(fs, 16)
         z = rep * 2 + half
@@ -174,16 +191,44 @@
         return pltpu.make_async_remote_copy(
             src_ref=ref,
             dst_ref=ref,
-            send_sem=self.send.at[k],
-            recv_sem=self.recv.at[k],
+            send_sem=self.send.at[send_unit(edge)],
+            recv_sem=self.recv.at[self.unit[unit_of(edge)]],
             device_id=self.device[edge["way"]],
             device_id_type=MESH,
         )
 
+    def whole(self, edge, at):
+        start, width = edge["columns"]
+        ref = self.buffers[edge["buffer"]].at[(*at, slice(None), pl.ds(start, width))]
+        return pltpu.make_async_remote_copy(
+            src_ref=ref,
+            dst_ref=ref,
+            send_sem=self.send.at[send_unit(edge)],
+            recv_sem=self.recv.at[self.unit[unit_of(edge)]],
+            device_id=self.device[edge["way"]],
+            device_id_type=MESH,
+        )
+
+    def wait_unit(self, k):
+        edge = self.edges[k]
+        unit, every = unit_of(edge), pl.ds(0, 4)
+        if unit == edge["key"]:
+            self.copy(k, True).wait_recv()
+        elif unit[2] == "z":
+            self.whole(edge, (self.z["other"], self.y[unit[3]] if len(unit) > 3 else every, every)).wait_recv()
+        elif unit[1] == 2:
+            self.whole(edge, (pl.ds(0, 2), self.y[2], every)).wait_recv()
+        else:
+            self.whole(edge, (pl.ds(0, 2), every, self.x[2])).wait_recv()
+
     def arrivals(self, ks):
-        found = [k for k in ks if k not in self.seen]
-        self.seen.update(found)
-        return [(True, k) for k in found]
+        found = []
+        for k in ks:
+            unit = unit_of(self.edges[k])
+            if unit not in self.seen:
+                self.seen.add(unit)
+                found.append((True, k))
+        return found
 
     def begin(self, k):
         return self.arrivals([self.index[p] for p in self.edges[k]["parents"]]) + [(False, k)]
@@ -200,7 +245,7 @@
     def run(self, steps):
         for arriving, k in steps:
             if arriving:
-                self.copy(k, True).wait_recv()
+                self.wait_unit(k)
             else:
                 self.copy(k, False).start()
 
@@ -230,8 +275,19 @@
         ]
 
     def sent(self, group):
+        done = set()
         for k in self.members(group):
-            self.copy(k, False).wait_send()
+            edge = self.edges[k]
+            tree, level = edge["key"][1], edge["key"][2][0]
+            if send_unit(edge) in done:
+                continue
+            done.add(send_unit(edge))
+            half, y, x = self.z["own"], self.y[0], self.x[0]
+            if tree < 2:
+                at = {"p": (half, y, pl.ds(0, 3)), "q": (half, pl.ds(0, 3), pl.ds(0, 4)), "z": (half, pl.ds(0, 4), pl.ds(0, 4))}
+            else:
+                at = {"z": (half, y, x), "p": (pl.ds(0, 2), y, pl.ds(0, 3)), "q": (pl.ds(0, 2), pl.ds(0, 3), pl.ds(0, 4))}
+            self.whole(edge, at[level]).wait_send()
 
 
 def at_step(step, table, gather, sub=0):
@@ -281,15 +337,15 @@
     small_loads = [pltpu.make_async_copy(a, b, ssem.at[k]) for k, (a, b) in enumerate(zip(small, held))]
     (gain, taps, rate, admit, logit, mix_gain, ffn_gain, gate_taps, up_taps) = held
     loads = []
-    pieces = [(out_w, b1, 0, 0, 1024), (down, b3, 0, 0, 1408)]
+    pieces = [(out_w, b1, 2, 0, 0, 1024), (down, b3, 4, 0, 0, 1408)]
     for k in range(8):
-        pieces += [(lin, b0, k * 128, k * 256, 128), (branch, b0, k * 128, k * 256 + 128, 128)]
+        pieces += [(lin, b0, 1, k * 128, k * 256, 128), (branch, b0, 1, k * 128, k * 256 + 128, 128)]
     for k in range(11):
-        pieces += [(gate, b2, k * 128, k * 256, 128), (up, b2, k * 128, k * 256 + 128, 128)]
-    for k, (source, target, at, to, width) in enumerate(pieces):
+        pieces += [(gate, b2, 3, k * 128, k * 256, 128), (up, b2, 3, k * 128, k * 256 + 128, 128)]
+    for source, target, owner, at, to, width in pieces:
         loads.append(
             pltpu.make_async_copy(
-                source.at[:, pl.ds(at, width)], target.at[zl, y0, x0, :, pl.ds(to, width)], load.at[k + 1]
+                source.at[:, pl.ds(at, width)], target.at[zl, y0, x0, :, pl.ds(to, width)], load.at[owner]
             )
         )
     for one in loads:
@@ -301,8 +357,9 @@
     x_copy = pltpu.make_async_remote_copy(
         src_ref=x, dst_ref=full.at[tp], send_sem=xsem.at[0], recv_sem=xsem.at[1], device_id=partner, device_id_type=MESH
     )
-    for one in loads:
-        one.wait()
+    for k, buffer in enumerate((b0, b1, b2, b3)):
+        slot = buffer.at[zl, y0, x0]
+        pltpu.make_async_copy(slot, slot, load.at[k + 1]).wait()
     gather.pump(0.0)
     x_copy.start()
     x_load.start()
@@ -536,7 +593,7 @@
 ):
     edges = tree_edges()
     plan = planned(edges)
-    count = len(edges)
+    count, sends = len({unit_of(e) for e in edges}), 12 * len(GROUPS)
     any_space = pl.BlockSpec(memory_space=pl.ANY)
     operands = [
         stream_in[0],
@@ -579,7 +636,7 @@
             pltpu.VMEM((LEN, 1024), BF16),
             pltpu.VMEM((LEN + 8, BLOCK), F32),
             pltpu.VMEM((LEN + 8, BLOCK), F32),
-            dma((count,)), dma((count,)), dma((41,)), dma((len(small),)), dma((2,)), dma((8,)), dma((8,)), dma((4,)), dma((4,)),
+            dma((sends,)), dma((count,)), dma((5,)), dma((len(small),)), dma((2,)), dma((8,)), dma((8,)), dma((4,)), dma((4,)),
             dma((4,)),
         ],
         compiler_params=pltpu.CompilerParams(

time: 139 us -> 134 us (0.964)
  Pallas kernels: 136 us -> 131 us
    pallas_call x1, Pallas kernels: 136 us -> 131 us  [local(): pl.pallas_call(functools.partial(kernel, edges, plan), out_shape=jax.Shap...]
where the time goes in v3:
time: 134 us
  Pallas kernels  131 us (98%)
  local copies, waits for them, and re-layouts  2.67 us (2%)
    pallas_call x1, Pallas kernels, local(): pl.pallas_call(functools.partial(kernel, edges, plan), out_shape=jax.Shap...  131 us

profile of v3, /device:TPU:1, one launch (start us, length us, event | category | flops | bytes accessed | tf_op | source)
XLA Modules:
  0.0 133.8 jit_solution(3111241096281150049)
XLA Ops:
  0.0 131.2 %shard_map.154 = bf16[768,1024]{1,0:T(8,128)(2,1)} custom-call(bf16[768,1024]{1,0:T(8,128)(2,1)} %bitcast.9, f32[1,2048]{1,0:T(1,128)} %bitcast.12, bf16[64,1024]{1,0:T(8,128)(2,1)} %refs_2_.1, bf16[64,1024]{1,0:T(8,128)(2,1)} %refs_3_.1, f32[4,1024]{1,0:T(4,128)} %refs_4_.1, bf16[8,128,128]{2,1,0:T(8,128)(2,1)} %refs_5_.1, bf16[8,128,128]{2,1,0:T(8,128)(2,1)} %refs_6_.1, ...), custom_call_target="tpu_custom_call" | custom-call | tf_op jit(solution)/shard_map/pallas_call | solution.py:618
  131.2 2.7 %copy.18 = bf16[1,768,1024]{2,1,0:T(8,128)(2,1)} copy(bf16[1,768,1024]{2,1,0:T(8,128)(2,1)} %bitcast.8) | data formatting | bytes 3145728

commit v4 on v3

--- a/solution.py
+++ b/solution.py
@@ -390,7 +390,7 @@
         total = sum(jnp.sum(part * part, axis=-1, keepdims=True) for part in halves)
         factor = lax.rsqrt(total * (1.0 / 2048.0) + EPS)
         for h in range(2):
-            normed[h, rows, :] = (halves[h] * factor * scales[:, h * 1024 : h * 1024 + 1024]).astype(BF16)
+            normed[rows, h * 1024 : h * 1024 + 1024] = (halves[h] * factor * scales[:, h * 1024 : h * 1024 + 1024]).astype(BF16)
 
     table = gather.timetable(LEN // NORM_ROWS // 6, *NORM_PACE)
 
@@ -410,11 +410,8 @@
 
     def both(buffer, step):
         columns = pl.ds(pl.multiple_of(step * 256, 256), 256)
-        total = None
-        for h in range(2):
-            weights = buffer[h, :, :, :, columns].reshape(1024, 256)
-            part = jnp.dot(normed[h], weights, preferred_element_type=F32)
-            total = part if total is None else total + part
+        weights = buffer[:, :, :, :, columns].reshape(2048, 256)
+        total = jnp.dot(normed[...], weights, preferred_element_type=F32)
         return total.astype(BF16).astype(F32)
 
     table1 = gather.timetable(8, start + MIX_PACE[0], MIX_PACE[1], 4)
@@ -584,7 +581,7 @@
 MIX_PACE = (4.0, 3.0)
 OUT_PACE = (28.0, 0.8)
 NORM2_US = 37.0
-FFN_PACE = (4.0, 1.6)
+FFN_PACE = (3.0, 1.4)
 
 
 def local(
@@ -627,7 +624,7 @@
             pltpu.VMEM((2, 4, 4, SHARD_ROWS, 2816), BF16),
             pltpu.VMEM((2, 4, 4, SHARD_ROWS, 1408), BF16),
             pltpu.VMEM((2, LEN, 1024), BF16),
-            pltpu.VMEM((2, LEN, 1024), BF16),
+            pltpu.VMEM((LEN, 2048), BF16),
             pltpu.VMEM((LEN, 1024), BF16),
             pltpu.VMEM((2, 4, LEN, 256), BF16),
             pltpu.VMEM((2, 4, LEN, 256), BF16),

time: 134 us -> 133 us (level)
  no operation moved by 1% of the time
where the time goes in v4:
time: 133 us
  Pallas kernels  130 us (98%)
  local copies, waits for them, and re-layouts  2.67 us (2%)
    pallas_call x1, Pallas kernels, local(): pl.pallas_call(functools.partial(kernel, edges, plan), out_shape=jax.Shap...  130 us
    unnamed x1, local copies, waits for them, and re-layouts  2.67 us

profile of v4, /device:TPU:1, one launch (start us, length us, event | category | flops | bytes accessed | tf_op | source)
XLA Modules:
  0.0 133.1 jit_solution(8435208320925792111)
XLA Ops:
  0.0 130.4 %shard_map.154 = bf16[768,1024]{1,0:T(8,128)(2,1)} custom-call(bf16[768,1024]{1,0:T(8,128)(2,1)} %bitcast.9, f32[1,2048]{1,0:T(1,128)} %bitcast.12, bf16[64,1024]{1,0:T(8,128)(2,1)} %refs_2_.1, bf16[64,1024]{1,0:T(8,128)(2,1)} %refs_3_.1, f32[4,1024]{1,0:T(4,128)} %refs_4_.1, bf16[8,128,128]{2,1,0:T(8,128)(2,1)} %refs_5_.1, bf16[8,128,128]{2,1,0:T(8,128)(2,1)} %refs_6_.1, ...), custom_call_target="tpu_custom_call" | custom-call | tf_op jit(solution)/shard_map/pallas_call | solution.py:615
  130.4 2.7 %copy.18 = bf16[1,768,1024]{2,1,0:T(8,128)(2,1)} copy(bf16[1,768,1024]{2,1,0:T(8,128)(2,1)} %bitcast.8) | data formatting | bytes 3145728

commit v5 on v4

--- a/solution.py
+++ b/solution.py
@@ -318,7 +318,7 @@
 LEN = 768
 BLOCK = 128
 ROWS = 256
-NORM_ROWS = 16
+NORM_ROWS = 32
 
 
 def kernel(edges, plan, *refs):
@@ -392,15 +392,15 @@
         for h in range(2):
             normed[rows, h * 1024 : h * 1024 + 1024] = (halves[h] * factor * scales[:, h * 1024 : h * 1024 + 1024]).astype(BF16)
 
-    table = gather.timetable(LEN // NORM_ROWS // 6, *NORM_PACE)
-
-    @pl.loop(0, LEN // NORM_ROWS // 6)
+    table = gather.timetable(LEN // NORM_ROWS // 3, *NORM_PACE)
+
+    @pl.loop(0, LEN // NORM_ROWS // 3)
     def _(part):
         at_step(part, table, gather)
 
-        @pl.loop(0, 6)
+        @pl.loop(0, 3)
         def _(chunk):
-            norm(part * 6 + chunk, gain, False)
+            norm(part * 3 + chunk, gain, False)
 
     pad_a[0:8, :] = jnp.zeros((8, BLOCK), F32)
     pad_b[0:8, :] = jnp.zeros((8, BLOCK), F32)
@@ -480,15 +480,15 @@
     for j in range(8):
         arriving_copy(j).wait_recv()
 
-    table3 = gather.timetable(LEN // NORM_ROWS // 6, start + NORM2_US, NORM_PACE[1])
-
-    @pl.loop(0, LEN // NORM_ROWS // 6)
+    table3 = gather.timetable(LEN // NORM_ROWS // 3, start + NORM2_US, NORM_PACE[1])
+
+    @pl.loop(0, LEN // NORM_ROWS // 3)
     def _(part):
         at_step(part, table3, gather)
 
-        @pl.loop(0, 6)
+        @pl.loop(0, 3)
         def _(chunk):
-            norm(part * 6 + chunk, ffn_gain, True)
+            norm(part * 3 + chunk, ffn_gain, True)
 
     for j in range(8):
         out_copy(j).wait_send()

time: 133 us -> 133 us (level)
  no operation moved by 1% of the time
where the time goes in v5:
time: 133 us
  Pallas kernels  130 us (98%)
  local copies, waits for them, and re-layouts  2.67 us (2%)
    pallas_call x1, Pallas kernels, local(): pl.pallas_call(functools.partial(kernel, edges, plan), out_shape=jax.Shap...  130 us
    unnamed x1, local copies, waits for them, and re-layouts  2.67 us

profile of v5, /device:TPU:1, one launch (start us, length us, event | category | flops | bytes accessed | tf_op | source)
XLA Modules:
  0.0 132.6 jit_solution(18354189803324283348)
XLA Ops:
  0.0 129.9 %shard_map.154 = bf16[768,1024]{1,0:T(8,128)(2,1)} custom-call(bf16[768,1024]{1,0:T(8,128)(2,1)} %bitcast.9, f32[1,2048]{1,0:T(1,128)} %bitcast.12, bf16[64,1024]{1,0:T(8,128)(2,1)} %refs_2_.1, bf16[64,1024]{1,0:T(8,128)(2,1)} %refs_3_.1, f32[4,1024]{1,0:T(4,128)} %refs_4_.1, bf16[8,128,128]{2,1,0:T(8,128)(2,1)} %refs_5_.1, bf16[8,128,128]{2,1,0:T(8,128)(2,1)} %refs_6_.1, ...), custom_call_target="tpu_custom_call" | custom-call | tf_op jit(solution)/shard_map/pallas_call | solution.py:615
  129.9 2.7 %copy.18 = bf16[1,768,1024]{2,1,0:T(8,128)(2,1)} copy(bf16[1,768,1024]{2,1,0:T(8,128)(2,1)} %bitcast.8) | data formatting | bytes 3145728
